TPU v7x, 32 devices: a whole 2x2x4 slice. The times are simulated.
32 devices in a mesh: sp: 8 (over z, y), tp: 4 (over x, core).
Axes of the slice: x: 2, y: 2, z: 4, core: 2. Of those that a mesh axis runs over, the one named last changes fastest.
Arguments:
- tokens: bfloat16 [2560, 2048], P('sp', 'tp'), may hold values from -6 to 6
- pre_gain: float32 [2, 2048], replicated, may hold values from 0.1 to 1.9
- w_value: bfloat16 [2, 2048, 2048], P(None, 'sp', 'tp'), may hold values from -0.125 to 0.125
- w_gate: bfloat16 [2, 2048, 2048], P(None, 'sp', 'tp'), may hold values from -0.125 to 0.125
- taps: float32 [2, 31, 2048], P(None, None, 'tp'), may hold values from -5 to 5
- norm_gain: float32 [2, 2048], P(None, 'tp'), may hold values from 0.1 to 1.9
- norm_shift: float32 [2, 2048], P(None, 'tp'), may hold values from -3 to 3
- w_out: bfloat16 [2, 2048, 2048], P(None, 'tp', 'sp'), may hold values from -2 to 2
- post_gain: float32 [2, 2048], P(None, 'tp'), may hold values from 0.1 to 1.9
Outputs:
- stream: bfloat16 [2560, 2048], P('sp', 'tp')
All inputs are finite; a program needn't handle non-finite values.
Results may differ from a plain program's by a relative error of at most 0.015.
Values may be sent and summed in bfloat16 or wider, within the bound.
A program may use at most 64 MiB of HBM per device.

v0:
```python
import jax
import jax.numpy as jnp
from jax import lax
from jax.sharding import PartitionSpec as P

D = 2048
CONV_WIDTH = 31
LAYERS = 2


EPSILON = 1e-06
LN_EPSILON = 1e-05


def passed_along(block, axis, distance):
    devices = range(lax.axis_size(axis))
    route = [(i - distance, i) for i in devices if i - distance in devices]
    return lax.ppermute(block, axis, route)


def local(tokens, pre_gain, w_value, w_gate, taps, norm_gain, norm_shift, w_out, post_gain):
    stream = tokens
    full_value, full_gate = (
        lax.all_gather(w_value, "sp", axis=1, tiled=True),
        lax.all_gather(w_gate, "sp", axis=1, tiled=True),
    )
    full_out = lax.all_gather(w_out, "sp", axis=2, tiled=True)
    for layer in range(LAYERS):
        whole = lax.all_gather(stream, "tp", axis=1, tiled=True)
        whole_f = whole.astype(jnp.float32)
        normed = (
            whole_f
            * lax.rsqrt(jnp.mean(whole_f * whole_f, -1, keepdims=True) + EPSILON)
            * pre_gain[layer]
        ).astype(jnp.bfloat16)
        value_mat = full_value[layer]
        gate_mat = full_gate[layer]
        out_mat = full_out[layer]
        value_proj = jnp.dot(normed, value_mat, preferred_element_type=jnp.float32)
        gate_proj = jnp.dot(normed, gate_mat, preferred_element_type=jnp.float32)
        glu_act = (value_proj * jax.nn.sigmoid(gate_proj)).astype(jnp.bfloat16)
        rows = glu_act.shape[0]
        fringe = passed_along(glu_act[rows - (CONV_WIDTH - 1) :], "sp", 1)
        padded = jnp.concatenate([fringe, glu_act], 0).astype(jnp.float32)
        conv_out = jnp.zeros(glu_act.shape, jnp.float32)
        for offset in range(CONV_WIDTH):
            conv_out = conv_out + taps[layer, offset] * padded[offset : offset + rows]
        row_sum, row_square = lax.psum(
            (jnp.sum(conv_out, -1, keepdims=True), jnp.sum(conv_out * conv_out, -1, keepdims=True)),
            "tp",
        )
        center = row_sum / D
        spread = jnp.maximum(row_square / D - center * center, 0.0)
        activated = jax.nn.silu(
            (conv_out - center) * lax.rsqrt(spread + LN_EPSILON) * norm_gain[layer]
            + norm_shift[layer]
        ).astype(jnp.bfloat16)
        terms = jnp.dot(activated, out_mat, preferred_element_type=jnp.float32)
        summed = lax.psum_scatter(terms.astype(jnp.bfloat16), "tp", scatter_dimension=1, tiled=True)
        projected = summed.astype(jnp.float32)
        out_square = lax.psum(jnp.sum(projected * projected, -1, keepdims=True), "tp")
        scale = lax.rsqrt(out_square / D + EPSILON)
        stream = (stream.astype(jnp.float32) + projected * scale * post_gain[layer]).astype(
            jnp.bfloat16
        )
    return stream


def solution(mesh):
    placed = (
        P("sp", "tp"),
        P(),
        P(None, "sp", "tp"),
        P(None, "sp", "tp"),
        P(None, None, "tp"),
        P(None, "tp"),
        P(None, "tp"),
        P(None, "tp", "sp"),
        P(None, "tp"),
    )
    return jax.shard_map(
        local, mesh=mesh, in_specs=placed, out_specs=P("sp", "tp"), check_vma=False
    )
```

profile of v0, /device:TPU:0, one launch (start us, length us, event | category | flops | bytes accessed | tf_op | source)
XLA Modules:
  0.0 377.1 jit_solution(16301794310421925368)
XLA Ops:
  6.5 0.0 all-gather.6.cloned.1.call-start
  6.5 0.7 all-gather.6.cloned.1.call-update
  7.3 0.0 all-gather.10.cloned.1.call-start
  7.3 0.7 all-gather.10.cloned.1.call-update
  8.0 0.0 all-gather.8.cloned.1.call-start
  8.1 0.7 all-gather.8.cloned.1.call-update
  8.7 0.0 all-gather.12.cloned.1.call-start
  8.8 0.5 all-gather.12.cloned.1.call-update
  9.3 0.0 reduce-scatter.3.cloned.1.call-start
  9.4 0.8 fusion.116
  10.1 0.8 fusion.113
  10.9 0.9 fusion.112
  11.8 0.9 fusion.111
  12.7 0.8 fusion.114
  13.5 16.3 %all-gather.6.cloned.1.call-done = bf16[320,2048]{1,0:T(8,128)(2,1)} async-done(((bf16[320,512]{1,0:T(8,128)(2,1)}), bf16[320,2048]{1,0:T(8,128)(2,1)}) %all-gather.6.cloned.1.call-update) | async-done | bytes 1310736 | tf_op jit(solution)/shard_map/all_gather | solution.py:29
  29.8 1.7 fusion
  31.5 73.3 %all-gather.10.cloned.1.call-done = bf16[2,2048,512]{2,1,0:T(8,128)(2,1)} async-done(((bf16[2,256,512]{2,1,0:T(8,128)(2,1)}), bf16[2,2048,512]{2,1,0:T(8,128)(2,1)}) %all-gather.10.cloned.1.call-update) | async-done | bytes 4194320 | tf_op jit(solution)/shard_map/all_gather | solution.py:25
  104.8 0.0 copy-start.1
  104.8 3.1 fusion.20
  107.9 0.0 copy-start.4
  107.9 70.4 %all-gather.8.cloned.1.call-done = bf16[2,2048,512]{2,1,0:T(8,128)(2,1)} async-done(((bf16[2,256,512]{2,1,0:T(8,128)(2,1)}), bf16[2,2048,512]{2,1,0:T(8,128)(2,1)}) %all-gather.8.cloned.1.call-update) | async-done | bytes 4194320 | tf_op jit(solution)/shard_map/all_gather | solution.py:24
  178.3 0.0 copy-done.1
  178.3 2.5 fusion.19
  180.8 2.5 collective-permute-start
  183.3 0.0 copy-done.4
  183.3 1.6 collective-permute-done
  184.9 0.1 maximum_convert_fusion
  185.0 3.2 fusion.107
  188.2 6.1 %all-reduce.1 = (f32[320,1]{0,1:T(1,128)S(1)}, f32[320,1]{0,1:T(1,128)S(1)}) all-reduce(f32[320,1]{0,1:T(1,128)S(1)} %broadcast_in_dim.20, f32[320,1]{0,1:T(1,128)S(1)} %broadcast_in_dim.21), channel_id=1, replica_groups=mesh['sp'=8,'tp'=4] {'tp'}, use_global_device_ids=true, to_apply=%region_2.0 | all-reduce | flops 640 | bytes 5120 | tf_op jit(solution)/shard_map/psum | solution.py:48
  194.3 59.2 %all-gather.12.cloned.1.call-done = bf16[2,512,2048]{2,1,0:T(8,128)(2,1)} async-done(((bf16[2,512,256]{2,1,0:T(8,128)(2,1)}), bf16[2,512,2048]{2,1,0:T(8,128)(2,1)}) %all-gather.12.cloned.1.call-update) | async-done | bytes 4194320 | tf_op jit(solution)/shard_map/all_gather | solution.py:27
  253.4 0.0 copy-start.5
  253.4 0.0 copy-start.3
  253.5 3.8 %convolution_convert_fusion.1 = bf16[320,2048]{1,0:T(8,128)(2,1)} fusion(bf16[2,512,2048]{2,1,0:T(8,128)(2,1)} %all-gather.12.cloned.1.call-done, f32[320,512]{1,0:T(8,128)S(1)} %get-tuple-element.18, f32[512]{0:T(512)S(1)} %bitcast.183, f32[512]{0:T(512)S(1)} %bitcast.182, f32[320]{0:T(512)S(1)} %get-tuple-element.12, f32[320]{0:T(512)S(1)} %get-tuple-element.11), kind=kOutput, calls=%fused_computation.5 | convolution fusion | flops 673218560 | bytes 4069888 | tf_op jit(solution)/shard_map/dot_general | solution.py:58
  257.2 0.0 reduce-scatter.3.cloned.1.call-update
  257.3 0.0 all-gather.14.cloned.1.call-start
  257.3 0.0 copy-done.5
  257.3 24.7 %reduce-scatter.3.cloned.1.call-done = bf16[320,512]{1,0:T(8,128)(2,1)} async-done(((bf16[320,2048]{1,0:T(8,128)(2,1)}), bf16[320,512]{1,0:T(8,128)(2,1)}) %reduce-scatter.3.cloned.1.call-update) | async-done | bytes 327696 | tf_op jit(solution)/shard_map/reduce_scatter | solution.py:59
  282.0 1.1 fusion.22
  283.2 5.8 %psum.44 = f32[320,1]{0,1:T(1,128)S(1)} all-reduce(f32[320,1]{0,1:T(1,128)S(1)} %broadcast_in_dim.22), channel_id=1, replica_groups=mesh['sp'=8,'tp'=4] {'tp'}, use_global_device_ids=true, to_apply=%region_7.8 | all-reduce | flops 320 | bytes 2560 | tf_op jit(solution)/shard_map/psum | solution.py:61
  288.9 0.0 copy-done.3
  289.0 1.9 fusion.25
  290.8 0.0 all-gather.14.cloned.1.call-update
  290.9 0.0 reduce-scatter.5.cloned.1.call-start
  290.9 18.9 %all-gather.14.cloned.1.call-done = bf16[320,2048]{1,0:T(8,128)(2,1)} async-done(((bf16[320,512]{1,0:T(8,128)(2,1)}), bf16[320,2048]{1,0:T(8,128)(2,1)}) %all-gather.14.cloned.1.call-update) | async-done | bytes 1310736 | tf_op jit(solution)/shard_map/all_gather | solution.py:29
  309.8 1.7 fusion.3
  311.5 0.0 copy-start.2
  311.5 0.0 copy-start.6
  311.5 3.1 fusion.21
  314.6 0.0 copy-done.2
  314.6 0.5 copy-done.6
  315.1 0.9 fusion.18
  316.0 3.4 collective-permute-start.1
  319.4 0.9 fusion.110
  320.3 0.7 collective-permute-done.1
  321.0 0.1 maximum_convert_fusion.1
  321.1 3.2 fusion.106
  324.3 6.0 %all-reduce = (f32[320,1]{0,1:T(1,128)S(1)}, f32[320,1]{0,1:T(1,128)S(1)}) all-reduce(f32[320,1]{0,1:T(1,128)S(1)} %broadcast_in_dim.23, f32[320,1]{0,1:T(1,128)S(1)} %broadcast_in_dim.24), channel_id=1, replica_groups=mesh['sp'=8,'tp'=4] {'tp'}, use_global_device_ids=true, to_apply=%region_10.11 | all-reduce | flops 640 | bytes 5120 | tf_op jit(solution)/shard_map/psum | solution.py:48
  330.3 3.7 convolution_convert_fusion
  334.0 0.0 reduce-scatter.5.cloned.1.call-update
  334.0 27.4 %reduce-scatter.5.cloned.1.call-done = bf16[320,512]{1,0:T(8,128)(2,1)} async-done(((bf16[320,2048]{1,0:T(8,128)(2,1)}), bf16[320,512]{1,0:T(8,128)(2,1)}) %reduce-scatter.5.cloned.1.call-update) | async-done | bytes 327696 | tf_op jit(solution)/shard_map/reduce_scatter | solution.py:59
  361.4 1.1 fusion.26
  362.5 5.8 %psum.47 = f32[320,1]{0,1:T(1,128)S(1)} all-reduce(f32[320,1]{0,1:T(1,128)S(1)} %broadcast_in_dim.25), channel_id=1, replica_groups=mesh['sp'=8,'tp'=4] {'tp'}, use_global_device_ids=true, to_apply=%region_15.16 | all-reduce | flops 320 | bytes 2560 | tf_op jit(solution)/shard_map/psum | solution.py:61
  368.3 0.0 copy-done
  368.3 1.9 fusion.29
  (17 shorter events, 0.2 us)
Async XLA Ops:
  6.5 23.3 %all-gather.6.cloned.1.call-start = ((), (), s32[]{:S(2)}) async-start(), calls=%async_computation.2 | async-start | bytes 1638400 | tf_op jit(solution)/shard_map/all_gather | solution.py:29
  7.3 97.5 %all-gather.10.cloned.1.call-start = ((), (), s32[]{:S(2)}) async-start(), calls=%async_computation.4 | async-start | bytes 4718592 | tf_op jit(solution)/shard_map/all_gather | solution.py:25
  8.0 170.3 %all-gather.8.cloned.1.call-start = ((), (), s32[]{:S(2)}) async-start(), calls=%async_computation.3 | async-start | bytes 4718592 | tf_op jit(solution)/shard_map/all_gather | solution.py:24
  8.7 244.7 %all-gather.12.cloned.1.call-start = ((), (), s32[]{:S(2)}) async-start(), calls=%async_computation.5 | async-start | bytes 4718592 | tf_op jit(solution)/shard_map/all_gather | solution.py:27
  9.3 272.7 %reduce-scatter.3.cloned.1.call-start = ((), (), s32[]{:S(2)}) async-start(), calls=%async_computation.6 | async-start | bytes 1638400 | tf_op jit(solution)/shard_map/reduce_scatter | solution.py:59
  104.8 73.5 %copy-start.1 = (bf16[320,2048]{1,0:T(8,128)(2,1)S(1)}, bf16[320,2048]{1,0:T(8,128)(2,1)}, u32[]{:S(2)}) copy-start(bf16[320,2048]{1,0:T(8,128)(2,1)} %all-gather.6.cloned.1.call-done) | copy-start | bytes 3932164
  107.9 75.4 %copy-start.4 = (f32[2,512]{1,0:T(2,128)S(1)}, f32[2,512]{1,0:T(2,128)}, u32[]{:S(2)}) copy-start(f32[2,512]{1,0:T(2,128)} %param.15) | copy-start | bytes 12292
  180.8 4.0 %collective-permute-start = (bf16[30,512]{1,0:T(8,128)(2,1)S(1)}, bf16[30,512]{1,0:T(8,128)(2,1)S(1)}, u32[]{:S(2)}, u32[]{:S(2)}) collective-permute-start(bf16[30,512]{1,0:T(8,128)(2,1)S(1)} %slice.562), channel_id=1, source_target_pairs={{0,4},{4,8},{8,12},{12,16},{16,20},{20,24},{24,28},{1,5},{5,9},{9,... | collective-permute-start | bytes 92168 | tf_op jit(solution)/shard_map/ppermute | solution.py:18
  253.4 3.9 %copy-start.5 = (f32[2,512]{1,0:T(2,128)S(1)}, f32[2,512]{1,0:T(2,128)}, u32[]{:S(2)}) copy-start(f32[2,512]{1,0:T(2,128)} %param.17) | copy-start | bytes 12292
  253.4 35.5 %copy-start.3 = (bf16[320,512]{1,0:T(8,128)(2,1)S(1)}, bf16[320,512]{1,0:T(8,128)(2,1)}, u32[]{:S(2)}) copy-start(bf16[320,512]{1,0:T(8,128)(2,1)} %param.9) | copy-start | bytes 983044
  257.3 52.5 %all-gather.14.cloned.1.call-start = ((), (), s32[]{:S(2)}) async-start(), calls=%async_computation.7 | async-start | bytes 1638400 | tf_op jit(solution)/shard_map/all_gather | solution.py:29
  290.9 70.5 %reduce-scatter.5.cloned.1.call-start = ((), (), s32[]{:S(2)}) async-start(), calls=%async_computation.8 | async-start | bytes 1638400 | tf_op jit(solution)/shard_map/reduce_scatter | solution.py:59
  311.5 3.1 copy-start.2
  311.5 3.6 copy-start.6
  316.0 5.0 %collective-permute-start.1 = (bf16[30,512]{1,0:T(8,128)(2,1)S(1)}, bf16[30,512]{1,0:T(8,128)(2,1)S(1)}, u32[]{:S(2)}, u32[]{:S(2)}) collective-permute-start(bf16[30,512]{1,0:T(8,128)(2,1)S(1)} %slice.597), channel_id=1, source_target_pairs={{0,4},{4,8},{8,12},{12,16},{16,20},{20,24},{24,28},{1,5},{5,9},{9,... | collective-permute-start | bytes 92168 | tf_op jit(solution)/shard_map/ppermute | solution.py:18
  330.3 38.1 %copy-start = (bf16[320,512]{1,0:T(8,128)(2,1)S(1)}, bf16[320,512]{1,0:T(8,128)(2,1)}, u32[]{:S(2)}) copy-start(bf16[320,512]{1,0:T(8,128)(2,1)} %fusion.25) | copy-start | bytes 983044
Sparse Core Ops, SparseCore 0:
  8.9 20.8 all-gather.5
  32.0 72.7 all-gather.9
  107.0 71.2 all-gather.7
  180.2 73.1 all-gather.11
  257.4 24.5 reduce-scatter.2
  291.0 18.7 all-gather.13
  334.1 27.2 reduce-scatter.4
where the time goes:
time: 378 us; the launch traced here: 377 us
  waiting for transfers between devices  295 us (78%)
  blocking collectives  23.5 us (6%)
  matrix products  17 us (4%)
  other arithmetic  16 us (4%)
  between operations  13.7 us (4%)
  starting transfers between devices  6.07 us (2%)
  local copies, waits for them, and re-layouts  5.61 us (1%)
    all_gather x1, waiting for transfers between devices, local(): lax.all_gather(w_gate, 'sp', axis=1, tiled=True)  73.3 us
    all_gather x1, waiting for transfers between devices, local(): lax.all_gather(w_value, 'sp', axis=1, tiled=True)  70.4 us
    all_gather x1, waiting for transfers between devices, local(): full_out = lax.all_gather(w_out, 'sp', axis=2, tiled=True)  59.2 us
    reduce_scatter x2, waiting for transfers between devices, local(): lax.psum_scatter(terms.astype(jnp.bfloat16), 'tp', scatter_dimension=1, t...  52.1 us
    all_gather x2, waiting for transfers between devices, local(): whole = lax.all_gather(stream, 'tp', axis=1, tiled=True)  35.2 us
    psum x2, blocking collectives, local(): lax.psum((jnp.sum(conv_out, -1, keepdims=True), jnp.sum(conv_out * conv_o...  12 us
    psum x2, blocking collectives, local(): lax.psum(jnp.sum(projected * projected, -1, keepdims=True), 'tp')  11.5 us
  transfers between devices with their start and end apart: 9, of which 9 were waited for; matrix products, arithmetic and copies ran while one was open for 4% of the time, Pallas kernels for 0%

commit v1 on v0

--- a/solution.py
+++ b/solution.py
@@ -1,6 +1,10 @@
+import functools
+
 import jax
 import jax.numpy as jnp
 from jax import lax
+from jax.experimental import pallas as pl
+from jax.experimental.pallas import tpu as pltpu
 from jax.sharding import PartitionSpec as P
 
 D = 2048
@@ -66,7 +70,431 @@
     return stream
 
 
+TILE = 64
+HALO = 32
+TWICE = (2,)
+
+
+def step(
+    nz, x_ref, pre_ref, wv_hbm, wg_hbm, taps_ref, ng_ref, ns_ref, wo_hbm, post_ref, out_ref,
+    wvg, wo, whole, normed, glu, conv, act, part_out, part_in, cross_out, cross_in, total,
+    stat, stat_in, local_sem, su, ru, sd, rd, ys, yr, gs, gr, hs, hr, ss, sr, ps, pr, cs, cr,
+):
+    sp, tp = lax.axis_index("sp"), lax.axis_index("tp")
+    nsp, ntp = 2 * nz, 4
+    z, y = sp // 2, sp % 2
+    x, c = tp // 2, tp % 2
+    up, down, beside = (sp + 2, tp), (sp - 2, tp), (z * 2 + 1 - y, tp)
+    mate, across, diagonal = (sp, x * 2 + 1 - c), (sp, (1 - x) * 2 + c), (sp, (1 - x) * 2 + 1 - c)
+    rows, cols = x_ref.shape
+    layers = pre_ref.shape[0]
+    units = 3 * layers
+
+    def copy(src, dst, send, recv, to):
+        return pltpu.make_async_remote_copy(
+            src_ref=src, dst_ref=dst, send_sem=send, recv_sem=recv, device_id=to,
+            device_id_type=pl.DeviceIdType.MESH,
+        )
+
+    def piece(u, slot):
+        l, kind = divmod(u, 3)
+        if kind < 2:
+            depth = wv_hbm.shape[1]
+            return wvg.at[2 * l + kind, pl.ds(pl.multiple_of(slot * depth, depth), depth)]
+        depth = wo_hbm.shape[1]
+        return wo.at[l, pl.ds(pl.multiple_of(slot * depth, depth), depth)]
+
+    def lanes(u, yy):
+        return u + sum(t < u for t in TWICE) + yy
+
+    def sides(u):
+        return (0, 1) if u in TWICE else (0,)
+
+    def up_copy(u, yy, k):
+        i, p = lanes(u, yy), piece(u, (z - k) * 2 + (1 - y if yy else y))
+        return copy(p, p, su.at[i, k], ru.at[i, k], up)
+
+    def down_copy(u, yy, k):
+        i, p = lanes(u, yy), piece(u, (z + k) * 2 + (1 - y if yy else y))
+        return copy(p, p, sd.at[i, k], rd.at[i, k], down)
+
+    def beside_copy(u, oz):
+        p = piece(u, oz * 2 + y)
+        return copy(p, p, ys.at[u, oz], yr.at[u, oz], beside)
+
+    def beside_wait(u, oz):
+        p = piece(u, oz * 2 + 1 - y)
+        copy(p, p, ys.at[u, oz], yr.at[u, oz], beside).wait_recv()
+
+    def along(u, yy):
+        pl.when(z + 1 < nz)(lambda: up_copy(u, yy, 0).start())
+        pl.when(z > 0)(lambda: down_copy(u, yy, 0).start())
+
+    def own(u):
+        along(u, 0)
+        beside_copy(u, z).start()
+
+    def own_second(u):
+        beside_wait(u, z)
+        along(u, 1)
+
+    def relay(u, d):
+        for yy in sides(u):
+            i = lanes(u, yy)
+            side = 1 - y if yy else y
+
+            @pl.when(z >= d)
+            def _():
+                p = piece(u, (z - d) * 2 + side)
+                copy(p, p, su.at[i, d], ru.at[i, d - 1], beside).wait_recv()
+                pl.when(z + 1 < nz)(lambda: up_copy(u, yy, d).start())
+                if u not in TWICE:
+                    beside_copy(u, z - d).start()
+
+            @pl.when(z + d < nz)
+            def _():
+                p = piece(u, (z + d) * 2 + side)
+                copy(p, p, sd.at[i, d], rd.at[i, d - 1], beside).wait_recv()
+                pl.when(z > 0)(lambda: down_copy(u, yy, d).start())
+                if u not in TWICE:
+                    beside_copy(u, z + d).start()
+
+    def arrive(u):
+        if u not in TWICE:
+            for oz in range(nz):
+                beside_wait(u, oz)
+
+    def sent():
+        for u in range(units):
+            for yy in sides(u):
+                for k in range(nz - 1):
+                    pl.when((z >= k) & (z + 1 < nz))(lambda: up_copy(u, yy, k).wait_send())
+                    pl.when((z + k < nz) & (z > 0))(lambda: down_copy(u, yy, k).wait_send())
+            if u in TWICE:
+                beside_copy(u, z).wait_send()
+            else:
+                for oz in range(nz):
+                    beside_copy(u, oz).wait_send()
+
+    def gather(l):
+        b = whole.at[l, tp]
+        return (
+            copy(b, b, gs.at[l, 0], gr.at[l, 0], mate),
+            copy(b, b, gs.at[l, 1], gr.at[l, 1], across),
+        )
+
+    def gather_on(l):
+        b = whole.at[l, (1 - x) * 2 + c]
+        return copy(b, b, gs.at[l, 2], gr.at[l, 2], mate)
+
+    def gather_wait(l):
+        for j, t in ((0, x * 2 + 1 - c), (2, (1 - x) * 2 + 1 - c)):
+            b = whole.at[l, t]
+            copy(b, b, gs.at[l, j], gr.at[l, j], mate).wait_recv()
+
+    def gather_start(l):
+        for g in gather(l):
+            g.start()
+
+    def gather_turn(l):
+        b = whole.at[l, (1 - x) * 2 + c]
+        copy(b, b, gs.at[l, 1], gr.at[l, 1], across).wait_recv()
+        gather_on(l).start()
+
+    def norm(l):
+        gather_wait(l)
+
+        @pl.loop(0, rows // TILE)
+        def _(i):
+            r = pl.ds(pl.multiple_of(i * TILE, TILE), TILE)
+            square = jnp.zeros((TILE, 1), jnp.float32)
+            for t in range(ntp):
+                v = whole[l, t, r, :].astype(jnp.float32)
+                square = square + jnp.sum(v * v, -1, keepdims=True)
+            scale = lax.rsqrt(square / (cols * ntp) + EPSILON)
+            for t in range(ntp):
+                v = whole[l, t, r, :].astype(jnp.float32)
+                at = slice(t * cols, (t + 1) * cols)
+                normed[r, at] = (v * scale * pre_ref[l : l + 1, at]).astype(jnp.bfloat16)
+
+    def halo(l):
+        to = lax.rem(sp + 1, nsp)
+        return copy(
+            glu.at[l, pl.ds(rows, HALO)], glu.at[l, pl.ds(0, HALO)], hs.at[l], hr.at[l], (to, tp)
+        )
+
+    def project(l):
+        n = normed[...]
+        for j in range(cols // 256):
+            at = slice(j * 256, (j + 1) * 256)
+            value = jnp.dot(n, wvg[2 * l, :, at], preferred_element_type=jnp.float32)
+            gate = jnp.dot(n, wvg[2 * l + 1, :, at], preferred_element_type=jnp.float32)
+            glu[l, HALO:, at] = (value * jax.nn.sigmoid(gate)).astype(jnp.bfloat16)
+        pl.when(sp + 1 < nsp)(lambda: halo(l).start())
+
+    def exchange(e):
+        return [
+            copy(stat.at[e], stat_in.at[e, j], ss.at[e, j], sr.at[e, j], to)
+            for j, to in enumerate((mate, across, diagonal))
+        ]
+
+    def exchanged(e):
+        for s in exchange(e):
+            s.wait_recv()
+        return stat[e] + stat_in[e, 0] + stat_in[e, 1] + stat_in[e, 2]
+
+    lane = lax.broadcasted_iota(jnp.int32, (TILE, 128), 1)
+
+    def pick(sums, at):
+        return jnp.sum(jnp.where(lane == at, sums, 0.0), -1, keepdims=True)
+
+    def convolve(l):
+        @pl.when(sp == 0)
+        def _():
+            glu[l, :HALO] = jnp.zeros((HALO, cols), jnp.bfloat16)
+
+        pl.when(sp > 0)(lambda: halo(l).wait_recv())
+        first = HALO - (CONV_WIDTH - 1)
+
+        def tile(i, sums):
+            r = pl.multiple_of(i * TILE, TILE)
+            one = jnp.zeros((TILE, 128), jnp.float32)
+            two = jnp.zeros((TILE, 128), jnp.float32)
+            for j in range(cols // 128):
+                at = slice(j * 128, (j + 1) * 128)
+                window = glu[l, pl.ds(r, TILE + HALO), at].astype(jnp.float32)
+                acc = jnp.zeros((TILE, 128), jnp.float32)
+                for s in range(8):
+                    w = window if s == 0 else pltpu.roll(window, TILE + HALO - s, 0)
+                    for k in range(CONV_WIDTH):
+                        if (first + k) % 8 == s:
+                            o = first + k - s
+                            acc = acc + taps_ref[l, k : k + 1, at] * w[o : o + TILE]
+                conv[pl.ds(r, TILE), at] = acc
+                one = one + acc
+                two = two + acc * acc
+            sums = jnp.where(lane == 2 * i, jnp.sum(one, -1, keepdims=True), sums)
+            return jnp.where(lane == 2 * i + 1, jnp.sum(two, -1, keepdims=True), sums)
+
+        stat[2 * l] = lax.fori_loop(0, rows // TILE, tile, jnp.zeros((TILE, 128), jnp.float32))
+        for s in exchange(2 * l):
+            s.start()
+
+    def activate(l):
+        sums = exchanged(2 * l)
+
+        @pl.loop(0, rows // TILE)
+        def _(i):
+            r = pl.ds(pl.multiple_of(i * TILE, TILE), TILE)
+            center = pick(sums, 2 * i) / (cols * ntp)
+            spread = jnp.maximum(pick(sums, 2 * i + 1) / (cols * ntp) - center * center, 0.0)
+            v = (conv[r, :] - center) * lax.rsqrt(spread + LN_EPSILON)
+            v = v * ng_ref[l : l + 1, :] + ns_ref[l : l + 1, :]
+            act[r, :] = (v * jax.nn.sigmoid(v)).astype(jnp.bfloat16)
+
+    each = wo_hbm.shape[2]
+    per = cols // each
+    depth = wo_hbm.shape[1]
+
+    def term(l, t, h):
+        w = wo[l, pl.ds(pl.multiple_of((t * per + h) * depth, depth), depth), :]
+        return jnp.dot(act[...], w, preferred_element_type=jnp.float32).astype(jnp.bfloat16)
+
+    def pair(l, far, h):
+        i = far * per + h
+        return copy(part_out.at[l, i], part_in.at[l, i], ps.at[l, i], pr.at[l, i], mate)
+
+    def over(l, h):
+        return copy(cross_out.at[l, h], cross_in.at[l, h], cs.at[l, h], cr.at[l, h], across)
+
+    def give(l, far, h):
+        t = ((1 - x) if far else x) * 2 + 1 - c
+        part_out[l, far * per + h] = term(l, t, h)
+        pair(l, far, h).start()
+
+    def joined(l, far, h):
+        t = ((1 - x) if far else x) * 2 + c
+        mine = term(l, t, h).astype(jnp.float32)
+        pair(l, far, h).wait_recv()
+        return mine + part_in[l, far * per + h].astype(jnp.float32)
+
+    def reduce(l):
+        for h in range(per):
+            give(l, 1, h)
+        for h in range(per):
+            cross_out[l, h] = joined(l, 1, h).astype(jnp.bfloat16)
+            over(l, h).start()
+        for h in range(per):
+            give(l, 0, h)
+        for h in range(per):
+            total[:, h * each : (h + 1) * each] = joined(l, 0, h)
+
+    def finish(l):
+        for h in range(per):
+            over(l, h).wait_recv()
+
+        def tile(i, sums):
+            r = pl.ds(pl.multiple_of(i * TILE, TILE), TILE)
+            square = jnp.zeros((TILE, 1), jnp.float32)
+            for h in range(per):
+                at = slice(h * each, (h + 1) * each)
+                p = total[r, at] + cross_in[l, h, r, :].astype(jnp.float32)
+                p = p.astype(jnp.bfloat16).astype(jnp.float32)
+                total[r, at] = p
+                square = square + jnp.sum(p * p, -1, keepdims=True)
+            return jnp.where(lane == i, square, sums)
+
+        e = 2 * l + 1
+        stat[e] = lax.fori_loop(0, rows // TILE, tile, jnp.zeros((TILE, 128), jnp.float32))
+        for s in exchange(e):
+            s.start()
+        sums = exchanged(e)
+
+        @pl.loop(0, rows // TILE)
+        def _(i):
+            r = pl.ds(pl.multiple_of(i * TILE, TILE), TILE)
+            scale = lax.rsqrt(pick(sums, i) / (cols * ntp) + EPSILON)
+            old = whole[l, tp, r, :].astype(jnp.float32)
+            new = (old + total[r, :] * scale * post_ref[l : l + 1, :]).astype(jnp.bfloat16)
+            if l + 1 < layers:
+                whole[l + 1, tp, r, :] = new
+            else:
+                out_ref[r, :] = new
+
+    held = [pltpu.make_async_copy(x_ref, whole.at[0, tp], local_sem.at[units])]
+    for u in range(units):
+        l, kind = divmod(u, 3)
+        ref = (wv_hbm, wg_hbm, wo_hbm)[kind]
+        held.append(pltpu.make_async_copy(ref.at[l], piece(u, sp), local_sem.at[u]))
+    for h in held:
+        h.start()
+    barrier = pltpu.get_barrier_semaphore()
+    for i in range(1, nsp):
+        pl.semaphore_signal(
+            barrier, inc=1, device_id=(lax.rem(sp + i, nsp), tp),
+            device_id_type=pl.DeviceIdType.MESH,
+        )
+    for i in range(1, ntp):
+        pl.semaphore_signal(
+            barrier, inc=1, device_id=(sp, lax.rem(tp + i, ntp)),
+            device_id_type=pl.DeviceIdType.MESH,
+        )
+    pl.semaphore_wait(barrier, nsp + ntp - 2)
+    for h in held:
+        h.wait()
+
+    far = range(1, nz)
+    gather_start(0)
+    own(0)
+    own(1)
+    relay(0, 1)
+    gather_turn(0)
+    norm(0)
+    for d in far[1:]:
+        relay(0, d)
+    own(2)
+    for d in far:
+        relay(1, d)
+    own_second(2)
+    own(3)
+    arrive(0)
+    relay(2, 1)
+    arrive(1)
+    project(0)
+    relay(2, 2)
+    convolve(0)
+    for d in far[2:]:
+        relay(2, d)
+    activate(0)
+    own(4)
+    relay(3, 1)
+    arrive(2)
+    reduce(0)
+    relay(3, 2)
+    finish(0)
+    gather_start(1)
+    for d in far[2:]:
+        relay(3, d)
+    own(5)
+    relay(4, 1)
+    gather_turn(1)
+    norm(1)
+    for d in far[1:]:
+        relay(4, d)
+    arrive(3)
+    relay(5, 1)
+    arrive(4)
+    project(1)
+    relay(5, 2)
+    convolve(1)
+    for d in far[2:]:
+        relay(5, d)
+    activate(1)
+    arrive(5)
+    reduce(1)
+    finish(1)
+
+    sent()
+    for l in range(layers):
+        for g in (*gather(l), gather_on(l)):
+            g.wait_send()
+        pl.when(sp + 1 < nsp)(lambda: halo(l).wait_send())
+        for s in (*exchange(2 * l), *exchange(2 * l + 1)):
+            s.wait_send()
+        for h in range(per):
+            over(l, h).wait_send()
+            for side in (0, 1):
+                pair(l, side, h).wait_send()
+
+
+def kernel_local(nsp, *args):
+    tokens, pre_gain, w_value, _, _, _, _, w_out, _ = args
+    rows, cols = tokens.shape
+    layers, depth = w_value.shape[:2]
+    inner, each = w_out.shape[1:]
+    nz, units, per = nsp // 2, 3 * layers, cols // each
+    tracks = units + len(TWICE)
+    vmem, hbm = pl.BlockSpec(memory_space=pltpu.VMEM), pl.BlockSpec(memory_space=pl.ANY)
+    bf16, f32, dma = jnp.bfloat16, jnp.float32, pltpu.SemaphoreType.DMA
+    return pl.pallas_call(
+        functools.partial(step, nz),
+        out_shape=jax.ShapeDtypeStruct((rows, cols), bf16),
+        in_specs=[hbm, vmem, hbm, hbm, vmem, vmem, vmem, hbm, vmem],
+        out_specs=vmem,
+        scratch_shapes=[
+            pltpu.VMEM((2 * layers, nsp * depth, cols), bf16),
+            pltpu.VMEM((layers, nsp * inner, each), bf16),
+            pltpu.VMEM((layers, 4, rows, cols), bf16),
+            pltpu.VMEM((rows, 4 * cols), bf16),
+            pltpu.VMEM((layers, HALO + rows, cols), bf16),
+            pltpu.VMEM((rows, cols), f32),
+            pltpu.VMEM((rows, cols), bf16),
+            pltpu.VMEM((layers, 2 * per, rows, each), bf16),
+            pltpu.VMEM((layers, 2 * per, rows, each), bf16),
+            pltpu.VMEM((layers, per, rows, each), bf16),
+            pltpu.VMEM((layers, per, rows, each), bf16),
+            pltpu.VMEM((rows, cols), f32),
+            pltpu.VMEM((2 * layers, TILE, 128), f32),
+            pltpu.VMEM((2 * layers, 3, TILE, 128), f32),
+            dma((units + 1,)),
+            dma((tracks, nz)), dma((tracks, nz)), dma((tracks, nz)), dma((tracks, nz)),
+            dma((units, nz)), dma((units, nz)),
+            dma((layers, 3)), dma((layers, 3)),
+            dma((layers,)), dma((layers,)),
+            dma((2 * layers, 3)), dma((2 * layers, 3)),
+            dma((layers, 2 * per)), dma((layers, 2 * per)),
+            dma((layers, per)), dma((layers, per)),
+        ],
+        compiler_params=pltpu.CompilerParams(
+            collective_id=0, has_side_effects=True, vmem_limit_bytes=56 * 1024 * 1024
+        ),
+    )(*args)
+
+
 def solution(mesh):
+    nsp, ntp = mesh.shape["sp"], mesh.shape["tp"]
+    fits = nsp % 2 == 0 and 3 <= nsp // 2 <= 8 and ntp == 4 and D // nsp % 128 == 0
+    body = functools.partial(kernel_local, nsp) if fits else local
     placed = (
         P("sp", "tp"),
         P(),
@@ -79,5 +507,5 @@
         P(None, "tp"),
     )
     return jax.shard_map(
-        local, mesh=mesh, in_specs=placed, out_specs=P("sp", "tp"), check_vma=False
+        body, mesh=mesh, in_specs=placed, out_specs=P("sp", "tp"), check_vma=False
     )

time: 378 us -> 167 us (0.44)
  waiting for transfers between devices: 295 us -> 0 us
  Pallas kernels: 0 us -> 163 us
  blocking collectives: 23.5 us -> 0 us
  matrix products: 17 us -> 0 us
  other arithmetic: 16 us -> 0 us
  between operations: 13.7 us -> 0.01 us
  starting transfers between devices: 6.07 us -> 0 us
    all_gather x5 -> x0, waiting for transfers between devices: 238 us -> none  [the longest x1 73.3 us: local(): lax.all_gather(w_gate, 'sp', axis=1, tiled=True)]
    pallas_call x0 -> x1, Pallas kernels: none -> 163 us  [kernel_local(): pl.pallas_call(functools.partial(step, nz), out_shape=jax.ShapeDtypeStruc...]
    reduce_scatter x2 -> x0, waiting for transfers between devices: 52.1 us -> none  [local(): lax.psum_scatter(terms.astype(jnp.bfloat16), 'tp', scatter_dimension=1, t...]
    psum x4 -> x0, blocking collectives: 23.5 us -> none  [the longest x2 12 us: local(): lax.psum((jnp.sum(conv_out, -1, keepdims=True), jnp.sum(conv_out * conv_o...]
    dot_general x6 -> x0, matrix products: 17 us -> none  [the longest x2 7.48 us: local(): terms = jnp.dot(activated, out_mat, preferred_element_type=jnp.float32)]
    reduce_sum x6 -> x0, other arithmetic: 11.9 us -> none  [the longest x2 6.33 us: local(): jnp.sum(conv_out, -1, keepdims=True)]
    ppermute x2 -> x0, starting transfers between devices: 5.83 us -> none  [passed_along(): return lax.ppermute(block, axis, route)]
    slice x10 -> x0, local copies, waits for them, and re-layouts: 5.09 us -> none  [the longest x4 3.48 us: local(): conv_out = conv_out + taps[layer, offset] * padded[offset:offset + rows]]
  transfers between devices with their start and end apart: 9 -> 0, of which waited for: 9 -> 0; matrix products, arithmetic and copies ran while one was open for 4% -> 0% of each run, Pallas kernels for 0% -> 0%
where the time goes in v1:
time: 167 us; the launch traced here: 166 us
  Pallas kernels  163 us (98%)
  local copies, waits for them, and re-layouts  3.3 us (2%)
    pallas_call x1, Pallas kernels, kernel_local(): pl.pallas_call(functools.partial(step, nz), out_shape=jax.ShapeDtypeStruc...  163 us

profile of v1, /device:TPU:0, one launch (start us, length us, event | category | flops | bytes accessed | tf_op | source)
XLA Modules:
  0.0 166.5 jit_solution(6575549517277888559)
XLA Ops:
  0.0 1.6 copy.10.taps_ref
  1.6 163.2 %shard_map.91 = bf16[320,512]{1,0:T(8,128)(2,1)} custom-call(bf16[320,512]{1,0:T(8,128)(2,1)} %x_ref.1, f32[2,2048]{1,0:T(2,128)} %pre_ref.1, bf16[2,256,512]{2,1,0:T(8,128)(2,1)} %wv_hbm.1, bf16[2,256,512]{2,1,0:T(8,128)(2,1)} %wg_hbm.1, f32[2,31,512]{2,1,0:T(8,128)} %copy.10.taps_ref, f32[2,512]{1,0:T(2,128)} %ng_ref.1, f32[2,512]{1,0:T(2,128)} %ns_ref.1, ...), custom_call_target="tpu_custom_call" | custom-call | tf_op jit(solution)/shard_map/pallas_call | solution.py:459
  164.7 1.7 %copy.12 = bf16[320,512]{1,0:T(8,128)(2,1)} copy(bf16[320,512]{1,0:T(8,128)(2,1)} %shard_map.91) | data formatting | bytes 655360

commit v2 on v1

--- a/solution.py
+++ b/solution.py
@@ -72,13 +72,13 @@
 
 TILE = 64
 HALO = 32
-TWICE = (2,)
 
 
 def step(
     nz, x_ref, pre_ref, wv_hbm, wg_hbm, taps_ref, ng_ref, ns_ref, wo_hbm, post_ref, out_ref,
-    wvg, wo, whole, normed, glu, conv, act, part_out, part_in, cross_out, cross_in, total,
-    stat, stat_in, local_sem, su, ru, sd, rd, ys, yr, gs, gr, hs, hr, ss, sr, ps, pr, cs, cr,
+    wvg, other, wo, whole, normed, glu, conv, act, act_out, part_out, part_in, cross_out, cross_in,
+    total, taps, gain, shift, stat, stat_in, local_sem,
+    su, ru, sd, rd, ys, yr, gs, gr, hs, hr, ss, sr, ps, pr, cs, cr, acs, acr,
 ):
     sp, tp = lax.axis_index("sp"), lax.axis_index("tp")
     nsp, ntp = 2 * nz, 4
@@ -89,6 +89,9 @@
     rows, cols = x_ref.shape
     layers = pre_ref.shape[0]
     units = 3 * layers
+    both, half = 2 * rows, cols // 2
+    twice = [u for u in range(units) if u % 3 < 2]
+    mine = pl.ds(pl.multiple_of(y * half, half), half)
 
     def copy(src, dst, send, recv, to):
         return pltpu.make_async_remote_copy(
@@ -105,10 +108,10 @@
         return wo.at[l, pl.ds(pl.multiple_of(slot * depth, depth), depth)]
 
     def lanes(u, yy):
-        return u + sum(t < u for t in TWICE) + yy
+        return u + sum(t < u for t in twice) + yy
 
     def sides(u):
-        return (0, 1) if u in TWICE else (0,)
+        return (0, 1) if u in twice else (0,)
 
     def up_copy(u, yy, k):
         i, p = lanes(u, yy), piece(u, (z - k) * 2 + (1 - y if yy else y))
@@ -120,6 +123,9 @@
 
     def beside_copy(u, oz):
         p = piece(u, oz * 2 + y)
+        if u in twice:
+            l, kind = divmod(u, 3)
+            return copy(other.at[2 * l + kind], p, ys.at[u, oz], yr.at[u, oz], beside)
         return copy(p, p, ys.at[u, oz], yr.at[u, oz], beside)
 
     def beside_wait(u, oz):
@@ -148,7 +154,7 @@
                 p = piece(u, (z - d) * 2 + side)
                 copy(p, p, su.at[i, d], ru.at[i, d - 1], beside).wait_recv()
                 pl.when(z + 1 < nz)(lambda: up_copy(u, yy, d).start())
-                if u not in TWICE:
+                if u not in twice:
                     beside_copy(u, z - d).start()
 
             @pl.when(z + d < nz)
@@ -156,11 +162,11 @@
                 p = piece(u, (z + d) * 2 + side)
                 copy(p, p, sd.at[i, d], rd.at[i, d - 1], beside).wait_recv()
                 pl.when(z > 0)(lambda: down_copy(u, yy, d).start())
-                if u not in TWICE:
+                if u not in twice:
                     beside_copy(u, z + d).start()
 
     def arrive(u):
-        if u not in TWICE:
+        if u not in twice:
             for oz in range(nz):
                 beside_wait(u, oz)
 
@@ -170,78 +176,103 @@
                 for k in range(nz - 1):
                     pl.when((z >= k) & (z + 1 < nz))(lambda: up_copy(u, yy, k).wait_send())
                     pl.when((z + k < nz) & (z > 0))(lambda: down_copy(u, yy, k).wait_send())
-            if u in TWICE:
+            if u in twice:
                 beside_copy(u, z).wait_send()
             else:
                 for oz in range(nz):
                     beside_copy(u, oz).wait_send()
 
-    def gather(l):
-        b = whole.at[l, tp]
-        return (
-            copy(b, b, gs.at[l, 0], gr.at[l, 0], mate),
-            copy(b, b, gs.at[l, 1], gr.at[l, 1], across),
-        )
-
-    def gather_on(l):
-        b = whole.at[l, (1 - x) * 2 + c]
-        return copy(b, b, gs.at[l, 2], gr.at[l, 2], mate)
+    here, there = y * 4, (1 - y) * 4
+    opposite = (1 - x) * 2 + c
+
+    routes = dict(
+        across=(here + tp, across),
+        beside=(here + tp, beside),
+        mate=(here + tp, mate),
+        across_mate=(here + opposite, mate),
+        beside_across=(there + tp, across),
+        beside_mate=(there + tp, mate),
+        both_mate=(there + opposite, mate),
+    )
+
+    def gather(l, name):
+        k = list(routes).index(name)
+        t, to = routes[name]
+        b = whole.at[l, t]
+        return copy(b, b, gs.at[l, k], gr.at[l, k], to)
+
+    def came(l, k, t):
+        b = whole.at[l, t]
+        copy(b, b, gs.at[l, k], gr.at[l, k], mate).wait_recv()
+
+    def gather_start(l):
+        for name in ("across", "beside", "mate"):
+            gather(l, name).start()
+
+    def gather_turn(l):
+        came(l, 1, there + tp)
+        gather(l, "beside_across").start()
+        gather(l, "beside_mate").start()
+        came(l, 0, here + opposite)
+        gather(l, "across_mate").start()
+
+    def gather_last(l):
+        came(l, 4, there + opposite)
+        gather(l, "both_mate").start()
 
     def gather_wait(l):
-        for j, t in ((0, x * 2 + 1 - c), (2, (1 - x) * 2 + 1 - c)):
-            b = whole.at[l, t]
-            copy(b, b, gs.at[l, j], gr.at[l, j], mate).wait_recv()
-
-    def gather_start(l):
-        for g in gather(l):
-            g.start()
-
-    def gather_turn(l):
-        b = whole.at[l, (1 - x) * 2 + c]
-        copy(b, b, gs.at[l, 1], gr.at[l, 1], across).wait_recv()
-        gather_on(l).start()
+        pair_tp, pair_opposite = x * 2 + 1 - c, (1 - x) * 2 + 1 - c
+        came(l, 2, here + pair_tp)
+        came(l, 3, here + pair_opposite)
+        came(l, 5, there + pair_tp)
+        came(l, 6, there + pair_opposite)
 
     def norm(l):
         gather_wait(l)
-
-        @pl.loop(0, rows // TILE)
+        tiles = rows // TILE
+
+        @pl.loop(0, 2 * tiles)
         def _(i):
-            r = pl.ds(pl.multiple_of(i * TILE, TILE), TILE)
+            g, r = i // tiles * 4, pl.ds(pl.multiple_of(i % tiles * TILE, TILE), TILE)
+            to = pl.ds(pl.multiple_of(i * TILE, TILE), TILE)
             square = jnp.zeros((TILE, 1), jnp.float32)
             for t in range(ntp):
-                v = whole[l, t, r, :].astype(jnp.float32)
+                v = whole[l, g + t, r, :].astype(jnp.float32)
                 square = square + jnp.sum(v * v, -1, keepdims=True)
             scale = lax.rsqrt(square / (cols * ntp) + EPSILON)
             for t in range(ntp):
-                v = whole[l, t, r, :].astype(jnp.float32)
+                v = whole[l, g + t, r, :].astype(jnp.float32)
                 at = slice(t * cols, (t + 1) * cols)
-                normed[r, at] = (v * scale * pre_ref[l : l + 1, at]).astype(jnp.bfloat16)
+                normed[to, at] = (v * scale * pre_ref[l : l + 1, at]).astype(jnp.bfloat16)
 
     def halo(l):
-        to = lax.rem(sp + 1, nsp)
         return copy(
-            glu.at[l, pl.ds(rows, HALO)], glu.at[l, pl.ds(0, HALO)], hs.at[l], hr.at[l], (to, tp)
+            glu.at[l, pl.ds(both, HALO)], glu.at[l, pl.ds(0, HALO)], hs.at[l], hr.at[l], up
         )
 
     def project(l):
         n = normed[...]
-        for j in range(cols // 256):
-            at = slice(j * 256, (j + 1) * 256)
-            value = jnp.dot(n, wvg[2 * l, :, at], preferred_element_type=jnp.float32)
-            gate = jnp.dot(n, wvg[2 * l + 1, :, at], preferred_element_type=jnp.float32)
-            glu[l, HALO:, at] = (value * jax.nn.sigmoid(gate)).astype(jnp.bfloat16)
-        pl.when(sp + 1 < nsp)(lambda: halo(l).start())
+        value = jnp.dot(n, wvg[2 * l], preferred_element_type=jnp.float32)
+        gate = jnp.dot(n, wvg[2 * l + 1], preferred_element_type=jnp.float32)
+        glu[l, HALO:, :] = (value * jax.nn.sigmoid(gate)).astype(jnp.bfloat16)
+        pl.when(z + 1 < nz)(lambda: halo(l).start())
+
+    partner = z * 2 + 1 - y
+    peers = [mate, across, diagonal, beside]
+    peers += [(partner, mate[1]), (partner, across[1]), (partner, diagonal[1])]
 
     def exchange(e):
         return [
             copy(stat.at[e], stat_in.at[e, j], ss.at[e, j], sr.at[e, j], to)
-            for j, to in enumerate((mate, across, diagonal))
+            for j, to in enumerate(peers[: 3 if e % 2 else 7])
         ]
 
     def exchanged(e):
-        for s in exchange(e):
+        sums = stat[e]
+        for j, s in enumerate(exchange(e)):
             s.wait_recv()
-        return stat[e] + stat_in[e, 0] + stat_in[e, 1] + stat_in[e, 2]
+            sums = sums + stat_in[e, j]
+        return sums
 
     lane = lax.broadcasted_iota(jnp.int32, (TILE, 128), 1)
 
@@ -249,18 +280,18 @@
         return jnp.sum(jnp.where(lane == at, sums, 0.0), -1, keepdims=True)
 
     def convolve(l):
-        @pl.when(sp == 0)
+        @pl.when(z == 0)
         def _():
-            glu[l, :HALO] = jnp.zeros((HALO, cols), jnp.bfloat16)
-
-        pl.when(sp > 0)(lambda: halo(l).wait_recv())
+            glu[l, :HALO] = jnp.zeros((HALO, half), jnp.bfloat16)
+
+        pl.when(z > 0)(lambda: halo(l).wait_recv())
         first = HALO - (CONV_WIDTH - 1)
 
         def tile(i, sums):
             r = pl.multiple_of(i * TILE, TILE)
             one = jnp.zeros((TILE, 128), jnp.float32)
             two = jnp.zeros((TILE, 128), jnp.float32)
-            for j in range(cols // 128):
+            for j in range(half // 128):
                 at = slice(j * 128, (j + 1) * 128)
                 window = glu[l, pl.ds(r, TILE + HALO), at].astype(jnp.float32)
                 acc = jnp.zeros((TILE, 128), jnp.float32)
@@ -269,28 +300,44 @@
                     for k in range(CONV_WIDTH):
                         if (first + k) % 8 == s:
                             o = first + k - s
-                            acc = acc + taps_ref[l, k : k + 1, at] * w[o : o + TILE]
+                            acc = acc + taps[l, k : k + 1, at] * w[o : o + TILE]
                 conv[pl.ds(r, TILE), at] = acc
                 one = one + acc
                 two = two + acc * acc
             sums = jnp.where(lane == 2 * i, jnp.sum(one, -1, keepdims=True), sums)
             return jnp.where(lane == 2 * i + 1, jnp.sum(two, -1, keepdims=True), sums)
 
-        stat[2 * l] = lax.fori_loop(0, rows // TILE, tile, jnp.zeros((TILE, 128), jnp.float32))
+        stat[2 * l] = lax.fori_loop(0, both // TILE, tile, jnp.zeros((TILE, 128), jnp.float32))
         for s in exchange(2 * l):
             s.start()
 
     def activate(l):
         sums = exchanged(2 * l)
-
-        @pl.loop(0, rows // TILE)
-        def _(i):
-            r = pl.ds(pl.multiple_of(i * TILE, TILE), TILE)
-            center = pick(sums, 2 * i) / (cols * ntp)
-            spread = jnp.maximum(pick(sums, 2 * i + 1) / (cols * ntp) - center * center, 0.0)
+        tiles = rows // TILE
+
+        def tile(q, i, store):
+            at = q * tiles + i
+            r = pl.ds(pl.multiple_of(at * TILE, TILE), TILE)
+            center = pick(sums, 2 * at) / (cols * ntp)
+            spread = jnp.maximum(pick(sums, 2 * at + 1) / (cols * ntp) - center * center, 0.0)
             v = (conv[r, :] - center) * lax.rsqrt(spread + LN_EPSILON)
-            v = v * ng_ref[l : l + 1, :] + ns_ref[l : l + 1, :]
-            act[r, :] = (v * jax.nn.sigmoid(v)).astype(jnp.bfloat16)
+            v = v * gain[l : l + 1, :] + shift[l : l + 1, :]
+            store(pl.ds(pl.multiple_of(i * TILE, TILE), TILE), (v * jax.nn.sigmoid(v)).astype(jnp.bfloat16))
+
+        def give_away(r, v):
+            act_out[l, r, :] = v
+
+        def keep(r, v):
+            act[l, y, r, :] = v
+
+        pl.loop(0, tiles)(lambda i: tile(1 - y, i, give_away))
+        shared(l).start()
+        pl.loop(0, tiles)(lambda i: tile(y, i, keep))
+        b = act.at[l, 1 - y]
+        copy(b, b, acs.at[l], acr.at[l], beside).wait_recv()
+
+    def shared(l):
+        return copy(act_out.at[l], act.at[l, y], acs.at[l], acr.at[l], beside)
 
     each = wo_hbm.shape[2]
     per = cols // each
@@ -298,7 +345,9 @@
 
     def term(l, t, h):
         w = wo[l, pl.ds(pl.multiple_of((t * per + h) * depth, depth), depth), :]
-        return jnp.dot(act[...], w, preferred_element_type=jnp.float32).astype(jnp.bfloat16)
+        first = jnp.dot(act[l, 0], w[:half], preferred_element_type=jnp.float32)
+        second = jnp.dot(act[l, 1], w[half:], preferred_element_type=jnp.float32)
+        return (first + second).astype(jnp.bfloat16)
 
     def pair(l, far, h):
         i = far * per + h
@@ -314,9 +363,9 @@
 
     def joined(l, far, h):
         t = ((1 - x) if far else x) * 2 + c
-        mine = term(l, t, h).astype(jnp.float32)
+        kept = term(l, t, h).astype(jnp.float32)
         pair(l, far, h).wait_recv()
-        return mine + part_in[l, far * per + h].astype(jnp.float32)
+        return kept + part_in[l, far * per + h].astype(jnp.float32)
 
     def reduce(l):
         for h in range(per):
@@ -354,20 +403,31 @@
         def _(i):
             r = pl.ds(pl.multiple_of(i * TILE, TILE), TILE)
             scale = lax.rsqrt(pick(sums, i) / (cols * ntp) + EPSILON)
-            old = whole[l, tp, r, :].astype(jnp.float32)
+            old = whole[l, here + tp, r, :].astype(jnp.float32)
             new = (old + total[r, :] * scale * post_ref[l : l + 1, :]).astype(jnp.bfloat16)
             if l + 1 < layers:
-                whole[l + 1, tp, r, :] = new
+                whole[l + 1, here + tp, r, :] = new
             else:
                 out_ref[r, :] = new
 
-    held = [pltpu.make_async_copy(x_ref, whole.at[0, tp], local_sem.at[units])]
+    held = [pltpu.make_async_copy(x_ref, whole.at[0, here + tp], local_sem.at[units])]
     for u in range(units):
         l, kind = divmod(u, 3)
         ref = (wv_hbm, wg_hbm, wo_hbm)[kind]
-        held.append(pltpu.make_async_copy(ref.at[l], piece(u, sp), local_sem.at[u]))
+        if kind < 2:
+            part = ref.at[l, :, mine]
+            rest = ref.at[l, :, pl.ds(pl.multiple_of((1 - y) * half, half), half)]
+            i = 2 * l + kind
+            held.append(pltpu.make_async_copy(rest, other.at[i], local_sem.at[units + 1 + i]))
+        else:
+            part = ref.at[l]
+        held.append(pltpu.make_async_copy(part, piece(u, sp), local_sem.at[u]))
     for h in held:
         h.start()
+    for l in range(layers):
+        taps[l] = taps_ref[l, :, mine]
+        gain[l : l + 1] = ng_ref[l : l + 1, mine]
+        shift[l : l + 1] = ns_ref[l : l + 1, mine]
     barrier = pltpu.get_barrier_semaphore()
     for i in range(1, nsp):
         pl.semaphore_signal(
@@ -375,11 +435,12 @@
             device_id_type=pl.DeviceIdType.MESH,
         )
     for i in range(1, ntp):
-        pl.semaphore_signal(
-            barrier, inc=1, device_id=(sp, lax.rem(tp + i, ntp)),
-            device_id_type=pl.DeviceIdType.MESH,
-        )
-    pl.semaphore_wait(barrier, nsp + ntp - 2)
+        for at in (sp, partner):
+            pl.semaphore_signal(
+                barrier, inc=1, device_id=(at, lax.rem(tp + i, ntp)),
+                device_id_type=pl.DeviceIdType.MESH,
+            )
+    pl.semaphore_wait(barrier, nsp - 1 + 2 * (ntp - 1))
     for h in held:
         h.wait()
 
@@ -387,43 +448,46 @@
     gather_start(0)
     own(0)
     own(1)
+    own_second(0)
+    own_second(1)
     relay(0, 1)
     gather_turn(0)
+    for d in far[1:]:
+        relay(0, d)
+    gather_last(0)
+    own(2)
+    relay(1, 1)
     norm(0)
     for d in far[1:]:
-        relay(0, d)
-    own(2)
-    for d in far:
         relay(1, d)
-    own_second(2)
     own(3)
-    arrive(0)
+    own_second(3)
     relay(2, 1)
-    arrive(1)
     project(0)
     relay(2, 2)
     convolve(0)
     for d in far[2:]:
         relay(2, d)
+    own(4)
+    own_second(4)
+    relay(3, 1)
     activate(0)
-    own(4)
-    relay(3, 1)
+    relay(3, 2)
     arrive(2)
     reduce(0)
-    relay(3, 2)
-    finish(0)
-    gather_start(1)
     for d in far[2:]:
         relay(3, d)
     own(5)
     relay(4, 1)
+    finish(0)
+    gather_start(1)
+    relay(4, 2)
     gather_turn(1)
+    gather_last(1)
+    for d in far[2:]:
+        relay(4, d)
     norm(1)
-    for d in far[1:]:
-        relay(4, d)
-    arrive(3)
     relay(5, 1)
-    arrive(4)
     project(1)
     relay(5, 2)
     convolve(1)
@@ -436,9 +500,10 @@
 
     sent()
     for l in range(layers):
-        for g in (*gather(l), gather_on(l)):
-            g.wait_send()
-        pl.when(sp + 1 < nsp)(lambda: halo(l).wait_send())
+        for name in routes:
+            gather(l, name).wait_send()
+        pl.when(z + 1 < nz)(lambda: halo(l).wait_send())
+        shared(l).wait_send()
         for s in (*exchange(2 * l), *exchange(2 * l + 1)):
             s.wait_send()
         for h in range(per):
@@ -453,7 +518,7 @@
     layers, depth = w_value.shape[:2]
     inner, each = w_out.shape[1:]
     nz, units, per = nsp // 2, 3 * layers, cols // each
-    tracks = units + len(TWICE)
+    tracks, half = units + 2 * layers, cols // 2
     vmem, hbm = pl.BlockSpec(memory_space=pltpu.VMEM), pl.BlockSpec(memory_space=pl.ANY)
     bf16, f32, dma = jnp.bfloat16, jnp.float32, pltpu.SemaphoreType.DMA
     return pl.pallas_call(
@@ -462,28 +527,34 @@
         in_specs=[hbm, vmem, hbm, hbm, vmem, vmem, vmem, hbm, vmem],
         out_specs=vmem,
         scratch_shapes=[
-            pltpu.VMEM((2 * layers, nsp * depth, cols), bf16),
+            pltpu.VMEM((2 * layers, nsp * depth, half), bf16),
+            pltpu.VMEM((2 * layers, depth, half), bf16),
             pltpu.VMEM((layers, nsp * inner, each), bf16),
-            pltpu.VMEM((layers, 4, rows, cols), bf16),
-            pltpu.VMEM((rows, 4 * cols), bf16),
-            pltpu.VMEM((layers, HALO + rows, cols), bf16),
-            pltpu.VMEM((rows, cols), f32),
-            pltpu.VMEM((rows, cols), bf16),
+            pltpu.VMEM((layers, 8, rows, cols), bf16),
+            pltpu.VMEM((2 * rows, 4 * cols), bf16),
+            pltpu.VMEM((layers, HALO + 2 * rows, half), bf16),
+            pltpu.VMEM((2 * rows, half), f32),
+            pltpu.VMEM((layers, 2, rows, half), bf16),
+            pltpu.VMEM((layers, rows, half), bf16),
             pltpu.VMEM((layers, 2 * per, rows, each), bf16),
             pltpu.VMEM((layers, 2 * per, rows, each), bf16),
             pltpu.VMEM((layers, per, rows, each), bf16),
             pltpu.VMEM((layers, per, rows, each), bf16),
             pltpu.VMEM((rows, cols), f32),
+            pltpu.VMEM((layers, CONV_WIDTH, half), f32),
+            pltpu.VMEM((layers, half), f32),
+            pltpu.VMEM((layers, half), f32),
             pltpu.VMEM((2 * layers, TILE, 128), f32),
-            pltpu.VMEM((2 * layers, 3, TILE, 128), f32),
-            dma((units + 1,)),
+            pltpu.VMEM((2 * layers, 7, TILE, 128), f32),
+            dma((units + 1 + 2 * layers,)),
             dma((tracks, nz)), dma((tracks, nz)), dma((tracks, nz)), dma((tracks, nz)),
             dma((units, nz)), dma((units, nz)),
-            dma((layers, 3)), dma((layers, 3)),
+            dma((layers, 7)), dma((layers, 7)),
             dma((layers,)), dma((layers,)),
-            dma((2 * layers, 3)), dma((2 * layers, 3)),
+            dma((2 * layers, 7)), dma((2 * layers, 7)),
             dma((layers, 2 * per)), dma((layers, 2 * per)),
             dma((layers, per)), dma((layers, per)),
+            dma((layers,)), dma((layers,)),
         ],
         compiler_params=pltpu.CompilerParams(
             collective_id=0, has_side_effects=True, vmem_limit_bytes=56 * 1024 * 1024
@@ -493,7 +564,7 @@
 
 def solution(mesh):
     nsp, ntp = mesh.shape["sp"], mesh.shape["tp"]
-    fits = nsp % 2 == 0 and 3 <= nsp // 2 <= 8 and ntp == 4 and D // nsp % 128 == 0
+    fits = nsp % 2 == 0 and 3 <= nsp // 2 <= 8 and ntp == 4 and D // max(nsp, 2 * ntp) % 128 == 0
     body = functools.partial(kernel_local, nsp) if fits else local
     placed = (
         P("sp", "tp"),

time: 167 us -> 170 us (1.018)
  Pallas kernels: 163 us -> 167 us
    pallas_call x1, Pallas kernels: 163 us -> 167 us  [kernel_local(): pl.pallas_call(functools.partial(step, nz), out_shape=jax.ShapeDtypeStruc...]
where the time goes in v2:
time: 170 us
  Pallas kernels  167 us (98%)
  local copies, waits for them, and re-layouts  3.3 us (2%)
    pallas_call x1, Pallas kernels, kernel_local(): pl.pallas_call(functools.partial(step, nz), out_shape=jax.ShapeDtypeStruc...  167 us

profile of v2, /device:TPU:0, one launch (start us, length us, event | category | flops | bytes accessed | tf_op | source)
XLA Modules:
  0.0 170.1 jit_solution(7139111830131256697)
XLA Ops:
  0.0 1.6 copy.10.taps_ref
  1.6 166.8 %shard_map.91 = bf16[320,512]{1,0:T(8,128)(2,1)} custom-call(bf16[320,512]{1,0:T(8,128)(2,1)} %x_ref.1, f32[2,2048]{1,0:T(2,128)} %pre_ref.1, bf16[2,256,512]{2,1,0:T(8,128)(2,1)} %wv_hbm.1, bf16[2,256,512]{2,1,0:T(8,128)(2,1)} %wg_hbm.1, f32[2,31,512]{2,1,0:T(8,128)} %copy.10.taps_ref, f32[2,512]{1,0:T(2,128)} %ng_ref.1, f32[2,512]{1,0:T(2,128)} %ns_ref.1, ...), custom_call_target="tpu_custom_call" | custom-call | tf_op jit(solution)/shard_map/pallas_call | solution.py:524
  168.4 1.7 %copy.12 = bf16[320,512]{1,0:T(8,128)(2,1)} copy(bf16[320,512]{1,0:T(8,128)(2,1)} %shard_map.91) | data formatting | bytes 655360

commit v3 on v2

--- a/solution.py
+++ b/solution.py
@@ -71,6 +71,7 @@
 
 
 TILE = 64
+PACK = 16
 HALO = 32
 
 
@@ -193,16 +194,19 @@
         beside_across=(there + tp, across),
         beside_mate=(there + tp, mate),
         both_mate=(there + opposite, mate),
+        across_beside=(here + opposite, beside),
     )
+    upper, lower = pl.ds(0, rows // 2), pl.ds(rows // 2, rows // 2)
+    parts = dict(beside_across=upper, across_beside=lower)
 
     def gather(l, name):
         k = list(routes).index(name)
         t, to = routes[name]
-        b = whole.at[l, t]
+        b = whole.at[l, t, parts[name]] if name in parts else whole.at[l, t]
         return copy(b, b, gs.at[l, k], gr.at[l, k], to)
 
-    def came(l, k, t):
-        b = whole.at[l, t]
+    def came(l, k, t, part=pl.ds(0, rows)):
+        b = whole.at[l, t, part]
         copy(b, b, gs.at[l, k], gr.at[l, k], mate).wait_recv()
 
     def gather_start(l):
@@ -214,10 +218,12 @@
         gather(l, "beside_across").start()
         gather(l, "beside_mate").start()
         came(l, 0, here + opposite)
+        gather(l, "across_beside").start()
         gather(l, "across_mate").start()
 
     def gather_last(l):
-        came(l, 4, there + opposite)
+        came(l, 4, there + opposite, upper)
+        came(l, 7, there + opposite, lower)
         gather(l, "both_mate").start()
 
     def gather_wait(l):
@@ -274,10 +280,20 @@
             sums = sums + stat_in[e, j]
         return sums
 
-    lane = lax.broadcasted_iota(jnp.int32, (TILE, 128), 1)
+    lane = lax.broadcasted_iota(jnp.int32, (PACK, 128), 1)
+    groups = TILE // PACK
 
     def pick(sums, at):
-        return jnp.sum(jnp.where(lane == at, sums, 0.0), -1, keepdims=True)
+        found = [
+            jnp.sum(jnp.where(lane == at * groups + g, sums, 0.0), -1, keepdims=True)
+            for g in range(groups)
+        ]
+        return jnp.concatenate(found, 0)
+
+    def pack(sums, at, column):
+        for g in range(groups):
+            sums = jnp.where(lane == at * groups + g, column[g * PACK : (g + 1) * PACK], sums)
+        return sums
 
     def convolve(l):
         @pl.when(z == 0)
@@ -304,10 +320,10 @@
                 conv[pl.ds(r, TILE), at] = acc
                 one = one + acc
                 two = two + acc * acc
-            sums = jnp.where(lane == 2 * i, jnp.sum(one, -1, keepdims=True), sums)
-            return jnp.where(lane == 2 * i + 1, jnp.sum(two, -1, keepdims=True), sums)
-
-        stat[2 * l] = lax.fori_loop(0, both // TILE, tile, jnp.zeros((TILE, 128), jnp.float32))
+            sums = pack(sums, 2 * i, jnp.sum(one, -1, keepdims=True))
+            return pack(sums, 2 * i + 1, jnp.sum(two, -1, keepdims=True))
+
+        stat[2 * l] = lax.fori_loop(0, both // TILE, tile, jnp.zeros((PACK, 128), jnp.float32))
         for s in exchange(2 * l):
             s.start()
 
@@ -391,10 +407,10 @@
                 p = p.astype(jnp.bfloat16).astype(jnp.float32)
                 total[r, at] = p
                 square = square + jnp.sum(p * p, -1, keepdims=True)
-            return jnp.where(lane == i, square, sums)
+            return pack(sums, i, square)
 
         e = 2 * l + 1
-        stat[e] = lax.fori_loop(0, rows // TILE, tile, jnp.zeros((TILE, 128), jnp.float32))
+        stat[e] = lax.fori_loop(0, rows // TILE, tile, jnp.zeros((PACK, 128), jnp.float32))
         for s in exchange(e):
             s.start()
         sums = exchanged(e)
@@ -462,32 +478,32 @@
         relay(1, d)
     own(3)
     own_second(3)
+    project(0)
     relay(2, 1)
-    project(0)
+    convolve(0)
     relay(2, 2)
-    convolve(0)
+    activate(0)
     for d in far[2:]:
         relay(2, d)
     own(4)
     own_second(4)
     relay(3, 1)
-    activate(0)
-    relay(3, 2)
     arrive(2)
     reduce(0)
+    relay(3, 2)
     for d in far[2:]:
         relay(3, d)
     own(5)
-    relay(4, 1)
     finish(0)
     gather_start(1)
+    relay(4, 1)
+    gather_turn(1)
     relay(4, 2)
-    gather_turn(1)
-    gather_last(1)
     for d in far[2:]:
         relay(4, d)
+    gather_last(1)
+    relay(5, 1)
     norm(1)
-    relay(5, 1)
     project(1)
     relay(5, 2)
     convolve(1)
@@ -515,6 +531,8 @@
 def kernel_local(nsp, *args):
     tokens, pre_gain, w_value, _, _, _, _, w_out, _ = args
     rows, cols = tokens.shape
+    if rows % TILE or 4 * rows > PACK * 128:
+        return local(*args)
     layers, depth = w_value.shape[:2]
     inner, each = w_out.shape[1:]
     nz, units, per = nsp // 2, 3 * layers, cols // each
@@ -544,12 +562,12 @@
             pltpu.VMEM((layers, CONV_WIDTH, half), f32),
             pltpu.VMEM((layers, half), f32),
             pltpu.VMEM((layers, half), f32),
-            pltpu.VMEM((2 * layers, TILE, 128), f32),
-            pltpu.VMEM((2 * layers, 7, TILE, 128), f32),
+            pltpu.VMEM((2 * layers, PACK, 128), f32),
+            pltpu.VMEM((2 * layers, 7, PACK, 128), f32),
             dma((units + 1 + 2 * layers,)),
             dma((tracks, nz)), dma((tracks, nz)), dma((tracks, nz)), dma((tracks, nz)),
             dma((units, nz)), dma((units, nz)),
-            dma((layers, 7)), dma((layers, 7)),
+            dma((layers, 8)), dma((layers, 8)),
             dma((layers,)), dma((layers,)),
             dma((2 * layers, 7)), dma((2 * layers, 7)),
             dma((layers, 2 * per)), dma((layers, 2 * per)),

time: 170 us -> 159 us (0.935)
  Pallas kernels: 167 us -> 156 us
    pallas_call x1, Pallas kernels: 167 us -> 156 us  [kernel_local(): pl.pallas_call(functools.partial(step, nz), out_shape=jax.ShapeDtypeStruc...]
where the time goes in v3:
time: 159 us
  Pallas kernels  156 us (98%)
  local copies, waits for them, and re-layouts  3.3 us (2%)
    pallas_call x1, Pallas kernels, kernel_local(): pl.pallas_call(functools.partial(step, nz), out_shape=jax.ShapeDtypeStruc...  156 us
    unnamed x2, local copies, waits for them, and re-layouts  3.3 us

profile of v3, /device:TPU:0, one launch (start us, length us, event | category | flops | bytes accessed | tf_op | source)
XLA Modules:
  0.0 159.0 jit_solution(9726451933822765292)
XLA Ops:
  0.0 1.6 copy.10.taps_ref
  1.6 155.7 %shard_map.91 = bf16[320,512]{1,0:T(8,128)(2,1)} custom-call(bf16[320,512]{1,0:T(8,128)(2,1)} %x_ref.1, f32[2,2048]{1,0:T(2,128)} %pre_ref.1, bf16[2,256,512]{2,1,0:T(8,128)(2,1)} %wv_hbm.1, bf16[2,256,512]{2,1,0:T(8,128)(2,1)} %wg_hbm.1, f32[2,31,512]{2,1,0:T(8,128)} %copy.10.taps_ref, f32[2,512]{1,0:T(2,128)} %ng_ref.1, f32[2,512]{1,0:T(2,128)} %ns_ref.1, ...), custom_call_target="tpu_custom_call" | custom-call | tf_op jit(solution)/shard_map/pallas_call | solution.py:542
  157.3 1.7 %copy.12 = bf16[320,512]{1,0:T(8,128)(2,1)} copy(bf16[320,512]{1,0:T(8,128)(2,1)} %shard_map.91) | data formatting | bytes 655360
